TPU v7x, 32 devices: a whole 2x2x4 slice. The times are simulated.
32 devices in a mesh: sp: 8 (over z, x), tp: 4 (over y, core).
Axes of the slice: x: 2, y: 2, z: 4, core: 2. Of those that a mesh axis runs over, the one named last changes fastest.
Arguments:
- block_input: bfloat16 [2048, 2048], P('sp'), may hold values from -8 to 8
- queries: bfloat16 [2048, 1024], P('sp', 'tp'), may hold values from -6 to 6
- keys: bfloat16 [2048, 1024], P('sp', 'tp'), may hold values from -6 to 6
- w_value: bfloat16 [2048, 2048], P(None, 'tp'), may hold values from -0.125 to 0.125
- log_decay: float32 [2048, 1024], P('sp', 'tp'), as said below
- d_out: bfloat16 [2048, 2048], P('sp', 'tp'), may hold values from -0.125 to 0.125
Outputs:
- d_queries: bfloat16 [2048, 1024], P('sp', 'tp')
- d_keys: bfloat16 [2048, 1024], P('sp', 'tp')
- d_log_decay: float32 [2048, 1024], P('sp', 'tp')
- d_w_value: float32 [2048, 2048], P('sp', 'tp')
- row_norms: float32 [2048], P('sp')
Inputs may be any that keep to these rules, and one draw needn't show every extreme that they name: log_decay is negative; key channels differ in rate, and rates change along the sequence.
All inputs are finite; a program needn't handle non-finite values.
Results may differ from a plain program's by a relative error of at most 0.015.
Values sent between devices are 32-bit elements; how exact they have to be, the bound alone decides.
A program may use at most 64 MiB of HBM per device.

v0:
```python
import jax
import jax.numpy as jnp
from jax import lax
from jax.sharding import PartitionSpec as P

DK = 128
DV = 256


def carried_in(value, axis, join, neutral, backward):
    count, mine = (lax.axis_size(axis), lax.axis_index(axis))
    pieces = jax.tree.map(lambda part: lax.all_gather(part, axis), value)
    if backward:
        pieces = jax.tree.map(lambda part: part[::-1], pieces)
        mine = count - 1 - mine
    subtotal = jax.tree.map(
        lambda part, zero: jnp.full_like(part, 0) + jnp.asarray(zero, part.dtype), value, neutral
    )

    def turn(position, subtotal):
        longer = join(subtotal, jax.tree.map(lambda part: part[position], pieces))
        return jax.tree.map(lambda new, old: jnp.where(position < mine, new, old), longer, subtotal)

    return lax.fori_loop(0, count - 1, turn, subtotal)


def split_heads(array, block_len, width):
    length = array.shape[0]
    return array.reshape(length // block_len, block_len, -1, width).transpose(2, 0, 1, 3)


def merge_heads(array):
    return array.transpose(1, 2, 0, 3).reshape(array.shape[1] * array.shape[2], -1)


def narrow_product(form, left, right):
    return jnp.einsum(form, left, right, preferred_element_type=jnp.float32)


def state_product(form, left, right):
    return jnp.einsum(form, left.astype(jnp.float32), right, precision=lax.Precision.HIGHEST)


def carry_combine(earlier, later):
    return (earlier[0] * later[0], later[0][..., None] * earlier[1] + later[1])


def on_device(block_input, queries, keys, w_value, log_decay, d_out):
    q_scale = DK ** (-0.5)
    block_len = 32
    values = jnp.dot(block_input, w_value, preferred_element_type=jnp.float32).astype(jnp.bfloat16)
    q_heads = split_heads(queries, block_len, DK).astype(jnp.float32) * q_scale
    k_heads = split_heads(keys, block_len, DK).astype(jnp.float32)
    v_heads = split_heads(values, block_len, DV)
    g_heads = split_heads(log_decay, block_len, DK)
    o_grad = split_heads(d_out, block_len, DV)
    cumlog = jnp.cumsum(g_heads, axis=2)
    last_log = cumlog[:, :, -1, :]
    last_wide = last_log[:, :, None, :]
    log_total = jnp.sum(last_log, axis=1)
    span_decay = jnp.exp(log_total)
    block_decay = jnp.exp(last_log)
    before_log = jnp.cumsum(last_log, axis=1) - last_log
    after_log = log_total[:, None, :] - jnp.cumsum(last_log, axis=1)
    k_tail = jnp.exp(last_wide - cumlog)
    q_grown = (q_heads * jnp.exp(cumlog)).astype(jnp.bfloat16)
    k_shrunk = (k_heads * jnp.exp(-cumlog)).astype(jnp.bfloat16)
    k_tailed = (k_heads * k_tail).astype(jnp.bfloat16)
    increments = narrow_product("hbcd,hbcv->hbdv", k_tailed, v_heads)
    backwards = narrow_product("hbcd,hbcv->hbdv", q_grown, o_grad)

    def forward_step(carried, inputs):
        decay_block, grown = inputs
        return (decay_block[:, :, None] * carried + grown, carried)

    def backward_step(adjoint, inputs):
        decay_block, grown = inputs
        return (grown + decay_block[:, :, None] * adjoint, adjoint)

    zero_state = jnp.zeros_like(increments[:, 0])
    span_state, local_states = lax.scan(
        forward_step, zero_state, (jnp.moveaxis(block_decay, 1, 0), jnp.moveaxis(increments, 1, 0))
    )
    span_adjoint, local_adjoints = lax.scan(
        backward_step,
        zero_state,
        (jnp.moveaxis(block_decay, 1, 0), jnp.moveaxis(backwards, 1, 0)),
        reverse=True,
    )
    identity = (jnp.ones_like(span_decay), jnp.zeros_like(span_state))
    _, state_in = carried_in((span_decay, span_state), "sp", carry_combine, identity, False)
    _, adjoint_in = carried_in((span_decay, span_adjoint), "sp", carry_combine, identity, True)
    entering = jnp.moveaxis(local_states, 0, 1) + jnp.exp(before_log)[..., None] * state_in[:, None]
    from_right = (
        jnp.moveaxis(local_adjoints, 0, 1) + jnp.exp(after_log)[..., None] * adjoint_in[:, None]
    )
    span_end = span_state + span_decay[..., None] * state_in
    decay_carry = jnp.sum(adjoint_in * span_end, axis=-1)
    causal = jnp.tril(jnp.ones((block_len, block_len), jnp.float32))
    out_dots = (narrow_product("hbcv,hbsv->hbcs", o_grad, v_heads) * causal).astype(jnp.bfloat16)
    key_dots = (narrow_product("hbcd,hbsd->hbcs", q_grown, k_shrunk) * causal).astype(jnp.bfloat16)
    q_adjoint = jnp.exp(cumlog) * (
        state_product("hbcv,hbdv->hbcd", o_grad, entering)
        + narrow_product("hbcs,hbsd->hbcd", out_dots, k_shrunk)
    )
    k_grad = jnp.exp(-cumlog) * narrow_product(
        "hbcs,hbcd->hbsd", out_dots, q_grown
    ) + k_tail * state_product("hbsv,hbdv->hbsd", v_heads, from_right)
    v_grad = narrow_product("hbcs,hbcv->hbsv", key_dots, o_grad) + state_product(
        "hbsd,hbdv->hbsv", k_tailed, from_right
    )
    decay_terms = merge_heads(q_heads * q_adjoint - k_heads * k_grad)
    d_log_decay = (
        jnp.flip(jnp.cumsum(jnp.flip(decay_terms, 0), 0), 0) + decay_carry.reshape(-1)[None, :]
    )
    value_grad = merge_heads(v_grad).astype(jnp.bfloat16)
    d_w_value = lax.psum_scatter(
        lax.dot_general(
            block_input, value_grad, (((0,), (0,)), ((), ())), preferred_element_type=jnp.float32
        ),
        "sp",
        scatter_dimension=0,
        tiled=True,
    )
    row_norms = lax.psum(jnp.sum(d_w_value * d_w_value, axis=1), "tp")
    d_queries = merge_heads(q_adjoint * q_scale).astype(jnp.bfloat16)
    d_keys = merge_heads(k_grad).astype(jnp.bfloat16)
    return (d_queries, d_keys, d_log_decay, d_w_value, row_norms)


def solution(mesh):
    placed = (
        P("sp", None),
        P("sp", "tp"),
        P("sp", "tp"),
        P(None, "tp"),
        P("sp", "tp"),
        P("sp", "tp"),
    )
    return jax.shard_map(
        on_device,
        mesh=mesh,
        in_specs=placed,
        out_specs=(P("sp", "tp"), P("sp", "tp"), P("sp", "tp"), P("sp", "tp"), P("sp")),
        check_vma=False,
    )
```

profile of v0, /device:TPU:0, one launch (start us, length us, event | category | flops | bytes accessed | tf_op | source)
XLA Modules:
  0.0 243.9 jit_solution(16168716474378182778)
XLA Ops:
  7.2 1.2 reshape.98
  8.4 1.1 reshape.93
  9.5 1.1 reshape.91
  11.4 1.6 convert_multiply_fusion
  13.1 1.1 mul.199
  14.9 1.1 fusion.48
  16.0 1.8 convolution_bitcast_fusion.1
  17.8 1.6 broadcast.41.clone.1
  19.4 14.6 %while.60 = (s32[]{:T(128)}, f32[2,128,256]{2,1,0:T(8,128)S(1)}, f32[8,2,128,256]{3,2,1,0:T(8,128)}, f32[8,2,128,256]{3,2,0,1:T(8,128)}, f32[8,2,128]{2,1,0:T(2,128)S(1)}, /*index=5*/s32[]{:T(128)}, s32[]{:T(128)}, s32[]{:T(128)}) while((s32[]{:T(128)}, f32[2,128,256]{2,1,0:T(8,128)S(1)}, f32[8,2,128,256]{3,2,1,0:T(8,128)}, ...), condition=%wide.region_8.9_spmd.clone, body=%wide.region_7.8_spmd.clone.sunk | while | flops 262148 | bytes 1313920 | solution.py:84
  20.1 1.1 bitcast_add_fusion.15
  21.9 1.1 bitcast_add_fusion.15
  23.7 1.1 bitcast_add_fusion.15
  25.6 1.1 bitcast_add_fusion.15
  27.4 1.1 bitcast_add_fusion.15
  29.2 1.1 bitcast_add_fusion.15
  31.1 1.1 bitcast_add_fusion.15
  32.9 1.1 bitcast_add_fusion.15
  34.8 2.7 %convolution_convert_fusion = bf16[256,512]{1,0:T(8,128)(2,1)} fusion(bf16[256,2048]{1,0:T(8,128)(2,1)} %param.14, bf16[2048,512]{1,0:T(8,128)(2,1)S(1)} %copy-done), kind=kOutput, calls=%fused_computation.25 | convolution fusion | flops 537001984 | bytes 3407872 | tf_op jit(solution)/shard_map/dot_general | solution.py:51
  37.5 1.0 reshape.92
  38.5 1.8 convolution_bitcast_fusion.2
  40.3 1.6 broadcast.41.clone
  41.9 14.6 %while.58 = (s32[]{:T(128)}, f32[2,128,256]{2,1,0:T(8,128)S(1)}, f32[8,2,128,256]{3,2,1,0:T(8,128)}, f32[8,2,128]{2,1,0:T(2,128)S(1)}, f32[8,2,128,256]{3,2,0,1:T(8,128)}, /*index=5*/s32[]{:T(128)}, s32[]{:T(128)}) while((s32[]{:T(128)}, f32[2,128,256]{2,1,0:T(8,128)S(1)}, f32[8,2,128,256]{3,2,1,0:T(8,128)}, ...), condition=%wide.region_2.3_spmd.clone, body=%wide.region_1.2_spmd.clone.sunk | while | flops 262147 | bytes 1313900 | solution.py:81
  42.6 1.1 bitcast_add_fusion.14
  44.4 1.1 bitcast_add_fusion.14
  46.3 1.1 bitcast_add_fusion.14
  48.1 1.1 bitcast_add_fusion.14
  49.9 1.1 bitcast_add_fusion.14
  51.7 1.1 bitcast_add_fusion.14
  53.5 1.1 bitcast_add_fusion.14
  55.4 1.1 bitcast_add_fusion.14
  57.8 22.5 %all-gather.3 = f32[8,2,128]{2,1,0:T(2,128)S(1)} all-gather(f32[1,2,128]{2,1,0:T(2,128)S(1)} %get-tuple-element.501), channel_id=2, replica_groups=mesh['sp'=8,'tp'=4] {'sp'}, dimensions={0}, use_global_device_ids=true | all-gather | bytes 9216 | tf_op jit(solution)/shard_map/all_gather | solution.py:12
  82.3 1.8 fusion.39
  84.1 2.7 %all-gather.9.cloned.1.call-done = f32[16,128,256]{2,1,0:T(8,128)} async-done(((f32[2,128,256]{2,1,0:T(8,128)}), f32[16,128,256]{2,1,0:T(8,128)}) %all-gather.9.cloned.1.call-update) | async-done | bytes 2097168 | tf_op jit(solution)/shard_map/all_gather | solution.py:12
  86.8 3.1 %rev.14 = f32[8,2,128,256]{3,2,1,0:T(8,128)} reverse(f32[8,2,128,256]{3,2,1,0:T(8,128)} %bitcast.185), dimensions={0} | reverse | bytes 4194304 | tf_op jit(solution)/shard_map/rev | solution.py:14
  89.9 12.2 %while.61 = (s32[]{:T(128)}, f32[2,128,256]{2,1,0:T(8,128)S(1)}, s32[]{:T(128)}, f32[8,2,128]{2,1,0:T(2,128)}, f32[8,2,128,256]{3,2,1,0:T(8,128)}, /*index=5*/s32[]{:T(128)}, s32[]{:T(128)}) while((s32[]{:T(128)}, f32[2,128,256]{2,1,0:T(8,128)S(1)}, s32[]{:T(128)}, f32[8,2,128]{2,1,0:T(2,128)}, f32[8,2,128,256]{3,2,1,0:T(8,128)}, ...), condition=%wide.region_10.11_spmd.clone, body=%wide.region_9.10_spmd.clone.sunk | while | flops 262148 | bytes 789617 | solution.py:24
  90.5 1.1 fusion.86
  92.3 1.1 fusion.86
  94.0 1.1 fusion.86
  95.7 1.1 fusion.86
  97.5 1.1 fusion.86
  99.3 1.1 fusion.86
  101.0 1.1 fusion.86
  102.1 2.8 %fusion.14 = bf16[8,32,2,256]{3,1,0,2:T(8,128)(2,1)S(1)} fusion(f32[2,8,32,256]{3,2,1,0:T(8,128)} %fusion.39, bf16[2,8,32,128]{3,1,2,0:T(8,128)(2,1)S(1)} %copy-done.9, f32[8,2,128,256]{3,2,1,0:T(8,128)} %get-tuple-element.328, f32[2,128,256]{2,1,0:T(8,128)S(1)} %get-tuple-element.330, f32[2,8,128]{2,0,1:T(2,128)S(1)} %copy.77), kind=kOutput, calls=%fused_computation.26 | convolution fusion | flops 202637312 | bytes 3284992 | tf_op jit(solution)/shard_map/hbsd,hbdv->hbsv/dot_general | solution.py:41
  105.2 2.7 %convolution_bitcast_fusion = f32[2048,512]{0,1:T(8,128)} fusion(bf16[256,512]{1,0:T(8,128)(2,1)S(1)} %bitcast.186, bf16[256,2048]{1,0:T(8,128)(2,1)S(1)} %copy-done.12), kind=kOutput, calls=%fused_computation.12 | convolution fusion | flops 536870912 | bytes 5505024 | tf_op jit(solution)/shard_map/dot_general | solution.py:118
  107.9 1.3 copy.66
  109.2 0.9 fusion.37
  110.2 1.8 convolution_bitcast_fusion.5
  112.0 0.9 fusion.36
  112.9 23.7 %all-gather.7.cloned.1.call-done = f32[16,128,256]{2,1,0:T(8,128)} async-done(((f32[2,128,256]{2,1,0:T(8,128)}), f32[16,128,256]{2,1,0:T(8,128)}) %all-gather.7.cloned.1.call-update) | async-done | bytes 2097168 | tf_op jit(solution)/shard_map/all_gather | solution.py:12
  136.6 7.8 %while.59 = (s32[]{:T(128)}, f32[2,128,256]{2,1,0:T(8,128)S(1)}, s32[]{:T(128)}, f32[8,2,128]{2,1,0:T(2,128)S(1)}, f32[8,2,128,256]{3,2,1,0:T(8,128)}, /*index=5*/s32[]{:T(128)}, s32[]{:T(128)}) while((s32[]{:T(128)}, f32[2,128,256]{2,1,0:T(8,128)S(1)}, s32[]{:T(128)}, f32[8,2,128]{2,1,0:T(2,128)S(1)}, ...), condition=%wide.region_6.7_spmd.clone, body=%wide.region_5.6_spmd.clone.sunk | while | flops 262148 | bytes 789617 | solution.py:24
  136.6 1.1 fusion.85
  137.7 1.1 fusion.85
  138.8 1.1 fusion.85
  140.0 1.1 fusion.85
  141.1 1.1 fusion.85
  142.2 1.1 fusion.85
  143.3 1.1 fusion.85
  144.5 3.5 %fusion.32 = f32[8,32,2,128]{3,1,0,2:T(8,128)S(1)} fusion(f32[8,32,2,128]{3,1,0,2:T(8,128)} %convolution_bitcast_fusion.5, f32[2,8,32,128]{3,1,2,0:T(8,128)S(1)} %fusion.52, bf16[8,32,2,256]{3,2,1,0:T(2,128)(2,1)S(1)} %reshape.93, f32[8,2,128,256]{3,2,1,0:T(8,128)} %get-tuple-element.325, f32[2,128,256]{2,1,0:T(8,128)S(1)} %get-tuple-element.327, ...), kind=kOutput, calls=%fused_computation.32 | convolution fusion | flops 202506240 | bytes 3416064 | tf_op jit(solution)/shard_map/hbcv,hbdv->hbcd/dot_general | solution.py:41
  148.1 1.5 fusion.56
  151.6 1.6 copy_bitcast_fusion.1
  153.9 73.6 %reduce-scatter.2.cloned.1.call-done = f32[256,512]{0,1:T(8,128)} async-done(((f32[2048,512]{0,1:T(8,128)}), f32[256,512]{0,1:T(8,128)}) %reduce-scatter.2.cloned.1.call-update) | async-done | bytes 524304 | tf_op jit(solution)/shard_map/reduce_scatter | solution.py:117
  227.5 1.1 multiply_reduce_fusion
  228.6 6.7 %psum.7 = f32[256]{0:T(256)} all-reduce(f32[256]{0:T(256)S(1)} %multiply_reduce_fusion), channel_id=1, replica_groups=mesh['sp'=8,'tp'=4] {'tp'}, use_global_device_ids=true, to_apply=%region_16.17 | all-reduce | flops 256 | bytes 2048 | tf_op jit(solution)/shard_map/psum | solution.py:125
  235.4 2.0 copy.91
  (118 shorter events, 24.9 us)
Async XLA Ops:
  7.2 27.6 %copy-start = (bf16[2048,512]{1,0:T(8,128)(2,1)S(1)}, bf16[2048,512]{1,0:T(8,128)(2,1)}, u32[]{:S(2)}) copy-start(bf16[2048,512]{1,0:T(8,128)(2,1)} %param.17) | copy-start | bytes 6291460
  7.2 79.6 %all-gather.9.cloned.1.call-start = ((), (), s32[]{:S(2)}) async-start(), calls=%async_computation.3 | async-start | bytes 2359296 | tf_op jit(solution)/shard_map/all_gather | solution.py:12
  8.4 9.4 %copy-start.5 = (f32[8,32,2,128]{3,2,1,0:T(2,128)}, f32[8,32,2,128]{3,2,1,0:T(2,128)S(1)}, u32[]{:S(2)}) copy-start(f32[8,32,2,128]{3,2,1,0:T(2,128)S(1)} %reshape.98) | copy-start | bytes 786436
  11.4 3.4 %copy-start.15 = (f32[2,128]{1,0:T(2,128)}, f32[2,128]{1,0:T(2,128)S(1)}, u32[]{:S(2)}) copy-start(f32[2,128]{1,0:T(2,128)S(1)} %get-tuple-element.494) | copy-start | bytes 3076
  14.2 5.2 %copy-start.7 = (f32[8,32,2,128]{3,2,1,0:T(2,128)}, f32[8,32,2,128]{3,2,1,0:T(2,128)S(1)}, u32[]{:S(2)}) copy-start(f32[8,32,2,128]{3,2,1,0:T(2,128)S(1)} %mul.199) | copy-start | bytes 786436
  34.0 0.7 copy-start.3
  34.7 101.9 %all-gather.7.cloned.1.call-start = ((), (), s32[]{:S(2)}) async-start(), calls=%async_computation.2 | async-start | bytes 2359296 | tf_op jit(solution)/shard_map/all_gather | solution.py:12
  34.8 3.7 %copy-start.9 = (bf16[2,8,32,128]{3,1,2,0:T(8,128)(2,1)S(1)}, bf16[2,8,32,128]{3,1,2,0:T(8,128)(2,1)}, u32[]{:S(2)}) copy-start(bf16[2,8,32,128]{3,1,2,0:T(8,128)(2,1)} %get-tuple-element.488) | copy-start | bytes 393220
  41.9 15.4 %copy-start.16 = (f32[2,128]{1,0:T(2,128)S(1)}, f32[2,128]{1,0:T(2,128)}, u32[]{:S(2)}) copy-start(f32[2,128]{1,0:T(2,128)} %copy-done.15) | copy-start | bytes 3076
  41.9 40.4 %copy-start.10 = (bf16[2,8,32,128]{3,1,2,0:T(8,128)(2,1)S(1)}, bf16[2,8,32,128]{3,1,2,0:T(8,128)(2,1)}, u32[]{:S(2)}) copy-start(bf16[2,8,32,128]{3,1,2,0:T(8,128)(2,1)} %get-tuple-element.489) | copy-start | bytes 393220
  56.5 0.7 copy-start.1
  57.2 170.3 %reduce-scatter.2.cloned.1.call-start = ((), (), s32[]{:S(2)}) async-start(), calls=%async_computation.1 | async-start | bytes 4718592 | tf_op jit(solution)/shard_map/reduce_scatter | solution.py:117
  102.1 3.1 %copy-start.12 = (bf16[256,2048]{1,0:T(8,128)(2,1)S(1)}, bf16[256,2048]{1,0:T(8,128)(2,1)}, u32[]{:S(2)}) copy-start(bf16[256,2048]{1,0:T(8,128)(2,1)} %param.14) | copy-start | bytes 3145732
  112.9 31.6 %copy-start.14 = (f32[2,8,128]{2,0,1:T(2,128)S(1)}, f32[2,8,128]{2,0,1:T(2,128)}, u32[]{:S(2)}) copy-start(f32[2,8,128]{2,0,1:T(2,128)} %copy.66) | copy-start | bytes 24580
  144.4 3.6 %copy-start.4 = (f32[8,2,128,256]{3,2,1,0:T(8,128)S(1)}, f32[8,2,128,256]{3,2,1,0:T(8,128)}, u32[]{:S(2)}) copy-start(f32[8,2,128,256]{3,2,1,0:T(8,128)} %get-tuple-element.328) | copy-start | bytes 6291460
  144.4 3.6 %copy-start.6 = (f32[8,32,2,128]{3,2,1,0:T(2,128)S(1)}, f32[8,32,2,128]{3,2,1,0:T(2,128)}, u32[]{:S(2)}) copy-start(f32[8,32,2,128]{3,2,1,0:T(2,128)} %copy-done.5) | copy-start | bytes 786436
  144.5 3.6 %copy-start.8 = (f32[8,32,2,128]{3,2,1,0:T(2,128)S(1)}, f32[8,32,2,128]{3,2,1,0:T(2,128)}, u32[]{:S(2)}) copy-start(f32[8,32,2,128]{3,2,1,0:T(2,128)} %copy-done.7) | copy-start | bytes 786436
  144.5 3.6 %copy-start.11 = (f32[8,32,2,128]{3,1,0,2:T(8,128)S(1)}, f32[8,32,2,128]{3,1,0,2:T(8,128)}, u32[]{:S(2)}) copy-start(f32[8,32,2,128]{3,1,0,2:T(8,128)} %fusion.36) | copy-start | bytes 786436
  144.5 3.6 %copy-start.13 = (f32[8,2,128]{2,0,1:T(8,128)S(1)}, f32[8,2,128]{2,0,1:T(8,128)}, u32[]{:S(2)}) copy-start(f32[8,2,128]{2,0,1:T(8,128)} %get-tuple-element.493) | copy-start | bytes 24580
  149.5 1.8 copy-start.2
  149.6 1.8 copy-start.17
Sparse Core Ops, SparseCore 0:
  34.9 51.8 all-gather.8
  88.9 47.6 all-gather.6
  140.2 87.2 reduce-scatter.1
where the time goes:
time: 246 us; the launch traced here: 244 us
  waiting for transfers between devices  100 us (41%)
  other arithmetic  51 us (21%)
  blocking collectives  29.3 us (12%)
  local copies, waits for them, and re-layouts  26.4 us (11%)
  matrix products  22.2 us (9%)
  between operations  14.2 us (6%)
    reduce_scatter x1, waiting for transfers between devices, on_device(): lax.psum_scatter(lax.dot_general(block_input, value_grad, (((0,), (0,)),...  73.6 us
    all_gather x2, waiting for transfers between devices, carried_in(): pieces = jax.tree.map(lambda part: lax.all_gather(part, axis), value)  26.4 us
    all_gather x1, blocking collectives, carried_in(): pieces = jax.tree.map(lambda part: lax.all_gather(part, axis), value)  22.5 us
    select_n x14, other arithmetic, turn(): jnp.where(position < mine, new, old)  15.1 us
    dynamic_update_slice x16, other arithmetic, on_device(): lax.scan(forward_step, zero_state, (jnp.moveaxis(block_decay, 1, 0), jnp....  11.7 us
    dot_general x6, matrix products, narrow_product(): return jnp.einsum(form, left, right, preferred_element_type=jnp.float32)  9.11 us
    add x8, other arithmetic, forward_step(): return (decay_block[:, :, None] * carried + grown, carried)  8.53 us
    add x8, other arithmetic, backward_step(): return (grown + decay_block[:, :, None] * adjoint, adjoint)  8.52 us
  transfers between devices with their start and end apart: 3, of which 3 were waited for; matrix products, arithmetic and copies ran while one was open for 28% of the time, Pallas kernels for 0%

commit v1 on v0

v1 whole, which is shorter than its diff:
```python
import functools

import jax
import jax.numpy as jnp
from jax import lax
from jax.experimental import pallas as pl
from jax.experimental.pallas import tpu as pltpu
from jax.sharding import PartitionSpec as P

DK = 128
DV = 256
BLOCK = 32
F32 = jnp.float32
BF16 = jnp.bfloat16
MESH = pl.DeviceIdType.MESH


def nn(left, right):
    return lax.dot_general(left, right, (((1,), (0,)), ((), ())), preferred_element_type=F32)


def nt(left, right):
    return lax.dot_general(left, right, (((1,), (1,)), ((), ())), preferred_element_type=F32)


def tn(left, right):
    return lax.dot_general(left, right, (((0,), (0,)), ((), ())), preferred_element_type=F32)


def pieces(value, count):
    parts = []
    for _ in range(count):
        part = value.astype(BF16)
        parts.append(part)
        value = value - part.astype(F32)
    return parts


def ring_place(z, x, nz, nx):
    r = nz - 1 - z
    across = jnp.where(r % 2 == 0, x - 1, nx - 1 - x)
    return jnp.where(x == 0, z, nz + r * (nx - 1) + across)


def ring_member(p, nz, nx):
    u = jnp.maximum(p - nz, 0)
    r = u // (nx - 1)
    w = u % (nx - 1)
    x = jnp.where(r % 2 == 0, 1 + w, nx - 1 - w)
    return jnp.where(p < nz, p * nx, (nz - 1 - r) * nx + x)


def kernel(
    n, nx, ntp,
    x_ref, q_ref, k_ref, w_ref, g_ref, o_ref,
    dq_ref, dk_ref, dg_ref, dw_ref, rn_ref,
    c_buf, span_buf, v_buf, qg_buf, kt_buf, ks_buf, y_buf, kp_buf, vp_buf, st_buf, xt_buf, vg_buf,
    a_out, a_in, z_out, z_in, z_acc, c_out, c_in, first, part, ring, norm_out, norm_in,
    a_send, a_recv, z_send, z_recv, c_send, c_recv, r_send, r_recv, n_send, n_recv,
):
    nz = n // nx
    me = lax.axis_index("sp")
    mine = lax.axis_index("tp")
    z, x = me // nx, me % nx
    tokens, heads = q_ref.shape[0], q_ref.shape[1] // DK
    blocks = tokens // BLOCK
    dvx = DV // nx
    scale = DK ** (-0.5)
    barrier = pltpu.get_barrier_semaphore()
    for off in range(1, n):
        pl.semaphore_signal(barrier, inc=1, device_id={"sp": (me + off) % n}, device_id_type=MESH)
    for off in range(1, ntp):
        pl.semaphore_signal(barrier, inc=1, device_id={"tp": (mine + off) % ntp}, device_id_type=MESH)

    row = lax.broadcasted_iota(jnp.int32, (tokens, tokens), 0)
    col = lax.broadcasted_iota(jnp.int32, (tokens, tokens), 1)
    below = col <= row
    inside = below & (col // BLOCK == row // BLOCK)
    tri = jnp.where(below, 1.0, 0.0).astype(BF16)
    tri_in = jnp.where(inside, 1.0, 0.0).astype(BF16)
    upper = jnp.where(col >= row, 1.0, 0.0).astype(BF16)
    last_in = jnp.where(col // BLOCK == row // BLOCK, 1.0, 0.0).astype(BF16)

    def hd(h):
        return slice(h * DK, (h + 1) * DK)

    def hv(h):
        return slice(h * DV, (h + 1) * DV)

    g_parts = pieces(g_ref[...], 3)
    span_buf[...] = sum(nn(tri, part_) for part_ in g_parts)
    c_buf[...] = sum(nn(tri_in, part_) for part_ in g_parts)
    total = span_buf[tokens - 1 : tokens, :]
    decay = jnp.exp(total)

    def scatter_copy(d, m):
        return pltpu.make_async_remote_copy(
            src_ref=a_out.at[d, m], dst_ref=a_in.at[d, x],
            send_sem=a_send.at[d, m], recv_sem=a_recv.at[d, x],
            device_id={"sp": z * nx + m}, device_id_type=MESH)

    def scatter_wait(d, m):
        pltpu.make_async_remote_copy(
            src_ref=a_out.at[d, m], dst_ref=a_in.at[d, m],
            send_sem=a_send.at[d, m], recv_sem=a_recv.at[d, m],
            device_id={"sp": z * nx + m}, device_id_type=MESH).wait_recv()

    def give(d, totals):
        for m in range(nx):
            for h in range(heads):
                a_out[d, m, h, :dvx, :] = totals[h][m * dvx : (m + 1) * dvx]
                a_out[d, m, h, dvx:, :] = jnp.broadcast_to(decay[:, hd(h)], (8, DK))
        for m in range(nx):
            @pl.when(m != x)
            def _():
                scatter_copy(d, m).start()

            @pl.when(m == x)
            def _():
                a_in[d, m] = a_out[d, m]

    q_all = q_ref[...].astype(F32) * scale
    q_span = (q_all * jnp.exp(span_buf[...])).astype(BF16)
    adjoints = [tn(o_ref[:, hv(h)], q_span[:, hd(h)]) for h in range(heads)]
    pl.semaphore_wait(barrier, n - 1 + ntp - 1)
    give(1, adjoints)

    for h in range(heads):
        v_buf[:, hv(h)] = nn(x_ref[...], w_ref[:, hv(h)]).astype(BF16)
    k_all = k_ref[...].astype(F32)
    k_far = jnp.exp(total - span_buf[...])
    k_span = (k_all * k_far).astype(BF16)
    states = [tn(v_buf[:, hv(h)], k_span[:, hd(h)]) for h in range(heads)]
    give(0, states)

    def plane(target):
        return {"sp": target * nx + x}

    def order(d):
        return range(nx) if d == 0 else range(nx - 1, -1, -1)

    def plane_copy(d, dz):
        return pltpu.make_async_remote_copy(
            src_ref=z_out.at[d], dst_ref=z_in.at[d, z],
            send_sem=z_send.at[d, dz], recv_sem=z_recv.at[d, z],
            device_id=plane(z + dz if d == 0 else z - dz), device_id_type=MESH)

    def plane_there(d, dz):
        return z + dz < nz if d == 0 else z - dz >= 0

    def combine(d):
        for m in range(nx):
            @pl.when(m != x)
            def _():
                scatter_wait(d, m)
        for h in range(heads):
            acc, dec = None, None
            for m in order(d):
                local, rate = a_in[d, m, h, :dvx, :], a_in[d, m, h, dvx:, :]
                acc = local if acc is None else local + rate[:1] * acc
                dec = rate if dec is None else rate * dec
            z_out[d, h, :dvx, :] = acc
            z_out[d, h, dvx:, :] = dec
        for dz in range(1, nz):
            @pl.when(plane_there(d, dz))
            def _():
                plane_copy(d, dz).start()

    combine(1)
    combine(0)

    cum = c_buf[...]
    block_end = sum(nn(last_in, part_) for part_ in g_parts)
    k_tail = jnp.exp(block_end - cum)
    grow = jnp.exp(cum)
    qg_buf[...] = (q_all * grow).astype(BF16)
    ks_buf[...] = (k_all * jnp.exp(-cum)).astype(BF16)
    kt_buf[...] = (k_all * k_tail).astype(BF16)
    st_buf[...] = jnp.zeros_like(st_buf)

    def span_step(step, carry):
        at = pl.multiple_of(step * BLOCK, BLOCK)
        back = pl.multiple_of((blocks - 1 - step) * BLOCK, BLOCK)
        rows, rows_b = pl.ds(at, BLOCK), pl.ds(back, BLOCK)
        for h in range(heads):
            keep = jnp.exp(c_buf[rows, hd(h)][BLOCK - 1 :])
            state = st_buf[0, h]
            y_buf[rows, hd(h)] = nn(o_ref[rows, hv(h)], state.astype(BF16))
            st_buf[0, h] = keep * state + tn(v_buf[rows, hv(h)], kt_buf[rows, hd(h)])
            keep = jnp.exp(c_buf[rows_b, hd(h)][BLOCK - 1 :])
            adjoint = st_buf[1, h]
            narrow = adjoint.astype(BF16)
            kp_buf[rows_b, hd(h)] = nn(v_buf[rows_b, hv(h)], narrow)
            vp_buf[rows_b, hv(h)] = nt(kt_buf[rows_b, hd(h)], narrow)
            st_buf[1, h] = keep * adjoint + tn(o_ref[rows_b, hv(h)], qg_buf[rows_b, hd(h)])
        return carry

    lax.fori_loop(0, blocks, span_step, 0)

    for h in range(heads):
        dots = jnp.where(inside, nt(o_ref[:, hv(h)], v_buf[:, hv(h)]), 0.0).astype(BF16)
        y_buf[:, hd(h)] += nn(dots, ks_buf[:, hd(h)])
        kp_buf[:, hd(h)] = (
            k_tail[:, hd(h)] * kp_buf[:, hd(h)]
            + jnp.exp(-cum[:, hd(h)]) * tn(dots, qg_buf[:, hd(h)])
        )
        dots = jnp.where(inside, nt(qg_buf[:, hd(h)], ks_buf[:, hd(h)]), 0.0).astype(BF16)
        vp_buf[:, hv(h)] += tn(dots, o_ref[:, hv(h)])

    depth = x_ref.shape[1]
    for at in range(0, depth, 256):
        xt_buf[at : at + 256, :] = x_ref[:, at : at + 256].T

    def member_copy(d, m):
        return pltpu.make_async_remote_copy(
            src_ref=c_out.at[d, m], dst_ref=c_in.at[d, x],
            send_sem=c_send.at[d, m], recv_sem=c_recv.at[d, x],
            device_id={"sp": z * nx + m}, device_id_type=MESH)

    def spread(d):
        z_acc[...] = jnp.zeros_like(z_acc)
        for zp in (range(nz) if d == 0 else range(nz - 1, -1, -1)):
            @pl.when(zp < z if d == 0 else zp > z)
            def _():
                pltpu.make_async_remote_copy(
                    src_ref=z_out.at[d], dst_ref=z_in.at[d, zp],
                    send_sem=z_send.at[d, 0], recv_sem=z_recv.at[d, zp],
                    device_id=plane(zp), device_id_type=MESH).wait_recv()
                for h in range(heads):
                    z_acc[h] = z_in[d, zp, h, :dvx, :] + z_in[d, zp, h, dvx : dvx + 1, :] * z_acc[h]
        for h in range(heads):
            acc = z_acc[h]
            for m in order(d):
                c_out[d, m, h] = acc
                acc = a_in[d, m, h, :dvx, :] + a_in[d, m, h, dvx : dvx + 1, :] * acc
        for m in range(nx):
            @pl.when(m != x)
            def _():
                member_copy(d, m).start()

            @pl.when(m == x)
            def _():
                c_in[d, m] = c_out[d, m]

    def entering(d):
        for m in range(nx):
            @pl.when(m != x)
            def _():
                pltpu.make_async_remote_copy(
                    src_ref=c_out.at[d, m], dst_ref=c_in.at[d, m],
                    send_sem=c_send.at[d, m], recv_sem=c_recv.at[d, m],
                    device_id={"sp": z * nx + m}, device_id_type=MESH).wait_recv()
        return [
            jnp.concatenate([c_in[d, m, h] for m in range(nx)], axis=0) for h in range(heads)
        ]

    spread(1)
    spread(0)
    from_right = entering(1)
    for h in range(heads):
        narrow = from_right[h].astype(BF16)
        vg_buf[:, hv(h)] = (vp_buf[:, hv(h)] + nt(k_span[:, hd(h)], narrow)).astype(BF16)

    own = dw_ref.shape[0]
    half_r, half_c = own // 2, dw_ref.shape[1] // 2
    p = ring_place(z, x, nz, nx)
    ahead = ring_member((p + 1) % n, nz, nx)
    behind = ring_member((p + n - 1) % n, nz, nx)

    def share(d, u, owner):
        rows_ = pl.ds(pl.multiple_of(owner * own + u * half_r, half_r), half_r)
        return nn(xt_buf[rows_, :], vg_buf[:, d * half_c : (d + 1) * half_c])

    def ring_copy(step, d, u, src):
        return pltpu.make_async_remote_copy(
            src_ref=src, dst_ref=ring.at[step, d, u],
            send_sem=r_send.at[step, d, u], recv_sem=r_recv.at[step, d, u],
            device_id={"sp": ahead if d == 0 else behind}, device_id_type=MESH)

    def owner_at(step, d):
        return ring_member((p + n - step - 1) % n if d == 0 else (p + step + 1) % n, nz, nx)

    for u in range(2):
        for d in range(2):
            first[d, u] = share(d, u, owner_at(0, d))
            ring_copy(0, d, u, first.at[d, u]).start()

    state_in = entering(0)
    for h in range(heads):
        k_grad = kp_buf[:, hd(h)] + k_far[:, hd(h)] * nn(v_buf[:, hv(h)], from_right[h].astype(BF16))
        dk_ref[:, hd(h)] = k_grad.astype(BF16)
        q_grad = grow[:, hd(h)] * y_buf[:, hd(h)] + jnp.exp(span_buf[:, hd(h)]) * nn(
            o_ref[:, hv(h)], state_in[h].astype(BF16)
        )
        dq_ref[:, hd(h)] = (q_grad * scale).astype(BF16)
        terms = q_all[:, hd(h)] * q_grad - k_all[:, hd(h)] * k_grad
        span_end = st_buf[0, h] + decay[:, hd(h)] * state_in[h]
        carry = jnp.sum(from_right[h] * span_end, axis=0, keepdims=True)
        dg_ref[:, hd(h)] = sum(nn(upper, part_) for part_ in pieces(terms, 3)) + carry

    def ring_step(step, carry):
        for d in range(2):
            for u in range(2):
                part[d, u] = share(d, u, owner_at(step, d))
        for u in range(2):
            for d in range(2):
                ring_copy(step - 1, d, u, first.at[d, u]).wait_recv()
                ring[step - 1, d, u] += part[d, u]
                ring_copy(step, d, u, ring.at[step - 1, d, u]).start()
        return carry

    lax.fori_loop(1, n - 1, ring_step, 0)

    for d in range(2):
        for u in range(2):
            part[d, u] = share(d, u, me)
    for u in range(2):
        squares = 0.0
        for d in range(2):
            ring_copy(n - 2, d, u, first.at[d, u]).wait_recv()
            done = ring[n - 2, d, u] + part[d, u]
            dw_ref[u * half_r : (u + 1) * half_r, d * half_c : (d + 1) * half_c] = done
            for at in range(0, half_c, 128):
                squares = squares + done[:, at : at + 128] * done[:, at : at + 128]
        norm_out[u] = jnp.broadcast_to(jnp.sum(squares.T, axis=0, keepdims=True), (8, half_r))

    def norm_copy(off):
        return pltpu.make_async_remote_copy(
            src_ref=norm_out, dst_ref=norm_in.at[off],
            send_sem=n_send.at[off], recv_sem=n_recv.at[off],
            device_id={"tp": (mine + off) % ntp}, device_id_type=MESH)

    for off in range(1, ntp):
        norm_copy(off).start()

    for d in range(2):
        for m in range(nx):
            @pl.when(m != x)
            def _():
                scatter_copy(d, m).wait_send()
                member_copy(d, m).wait_send()
        for dz in range(1, nz):
            @pl.when(plane_there(d, dz))
            def _():
                plane_copy(d, dz).wait_send()

    def sent(step, carry):
        for u in range(2):
            for d in range(2):
                ring_copy(step, d, u, first.at[d, u]).wait_send()
        return carry

    lax.fori_loop(0, n - 1, sent, 0)
    norms = norm_out[...]
    for off in range(1, ntp):
        norm_copy(off).wait()
        norms = norms + norm_in[off]
    rn_ref[...] = norms


def on_device(n, nx, ntp, block_input, queries, keys, w_value, log_decay, d_out):
    tokens, wide = queries.shape
    heads = wide // DK
    cols = w_value.shape[1]
    depth = block_input.shape[1]
    own = depth // n
    nz = n // nx
    dvx = DV // nx
    vm = pltpu.VMEM
    dma = pltpu.SemaphoreType.DMA
    out = pl.pallas_call(
        functools.partial(kernel, n, nx, ntp),
        out_shape=(
            jax.ShapeDtypeStruct((tokens, wide), BF16),
            jax.ShapeDtypeStruct((tokens, wide), BF16),
            jax.ShapeDtypeStruct((tokens, wide), F32),
            jax.ShapeDtypeStruct((own, cols), F32),
            jax.ShapeDtypeStruct((2, 8, own // 2), F32),
        ),
        in_specs=[pl.BlockSpec(memory_space=vm)] * 6,
        out_specs=(pl.BlockSpec(memory_space=vm),) * 5,
        scratch_shapes=[
            vm((tokens, wide), F32),
            vm((tokens, wide), F32),
            vm((tokens, cols), BF16),
            vm((tokens, wide), BF16),
            vm((tokens, wide), BF16),
            vm((tokens, wide), BF16),
            vm((tokens, wide), F32),
            vm((tokens, wide), F32),
            vm((tokens, cols), F32),
            vm((2, heads, DV, DK), F32),
            vm((depth, tokens), BF16),
            vm((tokens, cols), BF16),
            vm((2, nx, heads, dvx + 8, DK), F32),
            vm((2, nx, heads, dvx + 8, DK), F32),
            vm((2, heads, dvx + 8, DK), F32),
            vm((2, nz, heads, dvx + 8, DK), F32),
            vm((heads, dvx, DK), F32),
            vm((2, nx, heads, dvx, DK), F32),
            vm((2, nx, heads, dvx, DK), F32),
            vm((2, 2, own // 2, cols // 2), F32),
            vm((2, 2, own // 2, cols // 2), F32),
            vm((n - 1, 2, 2, own // 2, cols // 2), F32),
            vm((2, 8, own // 2), F32),
            vm((ntp, 2, 8, own // 2), F32),
            dma((2, nx)),
            dma((2, nx)),
            dma((2, nz)),
            dma((2, nz)),
            dma((2, nx)),
            dma((2, nx)),
            dma((n - 1, 2, 2)),
            dma((n - 1, 2, 2)),
            dma((ntp,)),
            dma((ntp,)),
        ],
        compiler_params=pltpu.CompilerParams(
            collective_id=0, has_side_effects=True, vmem_limit_bytes=56 * 1024 * 1024
        ),
    )(block_input, queries, keys, w_value, log_decay, d_out)
    return (*out[:4], out[4][:, 0].reshape(-1))


def solution(mesh):
    n, ntp = mesh.shape["sp"], mesh.shape["tp"]
    nx = 1 << ((n.bit_length() - 1) // 2)
    placed = (
        P("sp", None),
        P("sp", "tp"),
        P("sp", "tp"),
        P(None, "tp"),
        P("sp", "tp"),
        P("sp", "tp"),
    )
    return jax.shard_map(
        functools.partial(on_device, n, nx, ntp),
        mesh=mesh,
        in_specs=placed,
        out_specs=(P("sp", "tp"), P("sp", "tp"), P("sp", "tp"), P("sp", "tp"), P("sp")),
        check_vma=False,
    )
```

time: 246 us -> 84.8 us (0.34)
  waiting for transfers between devices: 100 us -> 0 us
  Pallas kernels: 0 us -> 76 us
  other arithmetic: 51 us -> 0 us
  blocking collectives: 29.3 us -> 0 us
  matrix products: 22.2 us -> 0 us
  local copies, waits for them, and re-layouts: 26.4 us -> 7.93 us
  between operations: 14.2 us -> 0.64 us
    pallas_call x0 -> x1, Pallas kernels: none -> 76 us  [on_device(): pl.pallas_call(functools.partial(kernel, n, nx, ntp), out_shape=(jax.Shap...]
    reduce_scatter x1 -> x0, waiting for transfers between devices: 73.6 us -> none  [on_device(): lax.psum_scatter(lax.dot_general(block_input, value_grad, (((0,), (0,)),...]
    all_gather x2 -> x0, waiting for transfers between devices: 26.4 us -> none  [carried_in(): pieces = jax.tree.map(lambda part: lax.all_gather(part, axis), value)]
    all_gather x1 -> x0, blocking collectives: 22.5 us -> none  [carried_in(): pieces = jax.tree.map(lambda part: lax.all_gather(part, axis), value)]
    dot_general x11 -> x0, matrix products: 22.2 us -> none  [the longest x6 9.11 us: narrow_product(): return jnp.einsum(form, left, right, preferred_element_type=jnp.float32)]
    add x17 -> x0, other arithmetic: 17.8 us -> none  [the longest x8 8.53 us: forward_step(): return (decay_block[:, :, None] * carried + grown, carried)]
    select_n x15 -> x0, other arithmetic: 15.7 us -> none  [the longest x14 15.1 us: turn(): jnp.where(position < mine, new, old)]
    dynamic_update_slice x16 -> x0, other arithmetic: 11.7 us -> none  [on_device(): lax.scan(forward_step, zero_state, (jnp.moveaxis(block_decay, 1, 0), jnp....]
  transfers between devices with their start and end apart: 3 -> 0, of which waited for: 3 -> 0; matrix products, arithmetic and copies ran while one was open for 28% -> 0% of each run, Pallas kernels for 0% -> 0%
where the time goes in v1:
time: 84.8 us; the launch traced here: 84.6 us
  Pallas kernels  76 us (90%)
  local copies, waits for them, and re-layouts  7.93 us (9%)
    pallas_call x1, Pallas kernels, on_device(): pl.pallas_call(functools.partial(kernel, n, nx, ntp), out_shape=(jax.Shap...  76 us
    unnamed x4, local copies, waits for them, and re-layouts  6.67 us

profile of v1, /device:TPU:0, one launch (start us, length us, event | category | flops | bytes accessed | tf_op | source)
XLA Modules:
  0.0 84.6 jit_solution(16452283667675776797)
XLA Ops:
  0.6 76.0 %shard_map.101 = (bf16[256,256]{1,0:T(8,128)(2,1)}, bf16[256,256]{1,0:T(8,128)(2,1)}, f32[256,256]{1,0:T(8,128)}, f32[256,512]{1,0:T(8,128)}, f32[2,8,128]{2,1,0:T(8,128)}) custom-call(bf16[256,2048]{1,0:T(8,128)(2,1)} %x_ref.1, bf16[256,256]{1,0:T(8,128)(2,1)} %q_ref.1, bf16[256,256]{1,0:T(8,128)(2,1)} %k_ref.1, bf16[2048,512]{1,0:T(8,128)(2,1)} %w_ref.1, ...), custom_call_target="tpu_custom_call" | custom-call | tf_op jit(solution)/shard_map/pallas_call | solution.py:371
  76.6 1.3 %slice.3 = f32[2,1,128]{2,1,0:T(1,128)} slice(f32[2,8,128]{2,1,0:T(8,128)} %get-tuple-element.14), slice={[0:2], [0:1], [0:128]} | slice | bytes 2048 | tf_op jit(solution)/shard_map/slice | solution.py:422
  77.9 1.6 %copy.15 = bf16[256,256]{1,0:T(8,128)(2,1)} copy(bf16[256,256]{1,0:T(8,128)(2,1)} %get-tuple-element.20) | data formatting | bytes 262144
  79.5 1.6 %copy.16 = bf16[256,256]{1,0:T(8,128)(2,1)} copy(bf16[256,256]{1,0:T(8,128)(2,1)} %get-tuple-element.21) | data formatting | bytes 262144
  81.0 1.7 %copy.17 = f32[256,256]{1,0:T(8,128)} copy(f32[256,256]{1,0:T(8,128)} %get-tuple-element.22) | data formatting | bytes 524288
  82.7 1.9 %copy.18 = f32[256,512]{1,0:T(8,128)} copy(f32[256,512]{1,0:T(8,128)} %get-tuple-element.23) | data formatting | bytes 1048576

commit v2 on v1

--- a/solution.py
+++ b/solution.py
@@ -356,6 +356,12 @@
         norm_copy(off).wait()
         norms = norms + norm_in[off]
     rn_ref[...] = norms
+
+
+def finish(*refs):
+    for source, target in zip(refs[:4], refs[5:9]):
+        target[...] = source[...]
+    refs[9][...] = refs[4][:, :1]
 
 
 def on_device(n, nx, ntp, block_input, queries, keys, w_value, log_decay, d_out):
@@ -416,10 +422,18 @@
             dma((ntp,)),
         ],
         compiler_params=pltpu.CompilerParams(
-            collective_id=0, has_side_effects=True, vmem_limit_bytes=56 * 1024 * 1024
+            collective_id=0, has_side_effects=True, vmem_limit_bytes=32 * 1024 * 1024
         ),
     )(block_input, queries, keys, w_value, log_decay, d_out)
-    return (*out[:4], out[4][:, 0].reshape(-1))
+    final = pl.pallas_call(
+        finish,
+        out_shape=tuple(jax.ShapeDtypeStruct(a.shape, a.dtype) for a in out[:4])
+        + (jax.ShapeDtypeStruct((2, 1, own // 2), F32),),
+        in_specs=[pl.BlockSpec(memory_space=vm)] * 5,
+        out_specs=(pl.BlockSpec(memory_space=vm),) * 5,
+        compiler_params=pltpu.CompilerParams(vmem_limit_bytes=8 * 1024 * 1024),
+    )(*out)
+    return (*final[:4], final[4].reshape(-1))
 
 
 def solution(mesh):

time: 84.8 us -> 81.4 us (0.960)
  Pallas kernels: 76 us -> 73.9 us
  local copies, waits for them, and re-layouts: 7.93 us -> 6.51 us
    pallas_call x1, Pallas kernels: 76 us -> 72.9 us  [on_device(): pl.pallas_call(functools.partial(kernel, n, nx, ntp), out_shape=(jax.Shap...]
    slice x1 -> x0, local copies, waits for them, and re-layouts: 1.26 us -> none  [on_device(): return (*out[:4], out[4][:, 0].reshape(-1))]
    pallas_call x0 -> x1, Pallas kernels: none -> 1.03 us  [on_device(): pl.pallas_call(finish, out_shape=tuple((jax.ShapeDtypeStruct(a.shape, a.d...]
    unnamed x4 -> x12, local copies, waits for them, and re-layouts: 6.67 us -> 6.51 us
where the time goes in v2:
time: 81.4 us; the launch traced here: 81.1 us
  Pallas kernels  73.9 us (91%)
  local copies, waits for them, and re-layouts  6.51 us (8%)
    pallas_call x1, Pallas kernels, on_device(): pl.pallas_call(functools.partial(kernel, n, nx, ntp), out_shape=(jax.Shap...  72.9 us
    unnamed x12, local copies, waits for them, and re-layouts  6.51 us

profile of v2, /device:TPU:0, one launch (start us, length us, event | category | flops | bytes accessed | tf_op | source)
XLA Modules:
  0.0 81.1 jit_solution(5210595692550395136)
XLA Ops:
  0.6 0.0 copy-start
  0.6 1.6 %copy-done = bf16[2048,512]{1,0:T(8,128)(2,1)S(1)} copy-done((bf16[2048,512]{1,0:T(8,128)(2,1)S(1)}, bf16[2048,512]{1,0:T(8,128)(2,1)}, u32[]{:S(2)}) %copy-start) | copy-done | bytes 2097176
  2.2 0.0 copy-start.1
  2.2 1.2 %copy-done.1 = bf16[256,2048]{1,0:T(8,128)(2,1)S(1)} copy-done((bf16[256,2048]{1,0:T(8,128)(2,1)S(1)}, bf16[256,2048]{1,0:T(8,128)(2,1)}, u32[]{:S(2)}) %copy-start.1) | copy-done | bytes 1048600
  3.5 0.0 copy-start.2
  3.5 0.9 %copy-done.2 = f32[256,256]{1,0:T(8,128)S(1)} copy-done((f32[256,256]{1,0:T(8,128)S(1)}, f32[256,256]{1,0:T(8,128)}, u32[]{:S(2)}) %copy-start.2) | copy-done | bytes 262168
  4.4 0.0 copy-start.3
  4.4 0.9 %copy-done.3 = bf16[256,512]{1,0:T(8,128)(2,1)S(1)} copy-done((bf16[256,512]{1,0:T(8,128)(2,1)S(1)}, bf16[256,512]{1,0:T(8,128)(2,1)}, u32[]{:S(2)}) %copy-start.3) | copy-done | bytes 262168
  5.4 0.0 copy-start.4
  5.4 0.9 %copy-done.4 = bf16[256,256]{1,0:T(8,128)(2,1)S(1)} copy-done((bf16[256,256]{1,0:T(8,128)(2,1)S(1)}, bf16[256,256]{1,0:T(8,128)(2,1)}, u32[]{:S(2)}) %copy-start.4) | copy-done | bytes 131096
  6.3 0.0 copy-start.5
  6.3 0.9 %copy-done.5 = bf16[256,256]{1,0:T(8,128)(2,1)S(1)} copy-done((bf16[256,256]{1,0:T(8,128)(2,1)S(1)}, bf16[256,256]{1,0:T(8,128)(2,1)}, u32[]{:S(2)}) %copy-start.5) | copy-done | bytes 131096
  7.2 72.9 %shard_map.101 = (bf16[256,256]{1,0:T(8,128)(2,1)S(1)}, bf16[256,256]{1,0:T(8,128)(2,1)S(1)}, f32[256,256]{1,0:T(8,128)S(1)}, f32[256,512]{1,0:T(8,128)S(1)}, f32[2,8,128]{2,1,0:T(8,128)S(1)}) custom-call(bf16[256,2048]{1,0:T(8,128)(2,1)S(1)} %copy-done.1, bf16[256,256]{1,0:T(8,128)(2,1)S(1)} %copy-done.4, bf16[256,256]{1,0:T(8,128)(2,1)S(1)} %copy-done.5, ...), custom_call_target="tpu_custom_call" | custom-call | tf_op jit(solution)/shard_map/pallas_call | solution.py:377
  80.1 1.0 %shard_map.102 = (bf16[256,256]{1,0:T(8,128)(2,1)}, bf16[256,256]{1,0:T(8,128)(2,1)}, f32[256,256]{1,0:T(8,128)}, f32[256,512]{1,0:T(8,128)}, f32[2,1,128]{2,1,0:T(1,128)}) custom-call(bf16[256,256]{1,0:T(8,128)(2,1)S(1)} %get-tuple-element.15.refs_0_, bf16[256,256]{1,0:T(8,128)(2,1)S(1)} %get-tuple-element.16.refs_1_, ...), custom_call_target="tpu_custom_call" | custom-call | tf_op jit(solution)/shard_map/pallas_call | solution.py:428
Async XLA Ops:
  0.6 1.6 %copy-start = (bf16[2048,512]{1,0:T(8,128)(2,1)S(1)}, bf16[2048,512]{1,0:T(8,128)(2,1)}, u32[]{:S(2)}) copy-start(bf16[2048,512]{1,0:T(8,128)(2,1)} %w_ref.1) | copy-start | bytes 6291460
  2.2 1.2 %copy-start.1 = (bf16[256,2048]{1,0:T(8,128)(2,1)S(1)}, bf16[256,2048]{1,0:T(8,128)(2,1)}, u32[]{:S(2)}) copy-start(bf16[256,2048]{1,0:T(8,128)(2,1)} %x_ref.1) | copy-start | bytes 3145732
  3.5 0.9 %copy-start.2 = (f32[256,256]{1,0:T(8,128)S(1)}, f32[256,256]{1,0:T(8,128)}, u32[]{:S(2)}) copy-start(f32[256,256]{1,0:T(8,128)} %g_ref.1) | copy-start | bytes 786436
  4.4 0.9 %copy-start.3 = (bf16[256,512]{1,0:T(8,128)(2,1)S(1)}, bf16[256,512]{1,0:T(8,128)(2,1)}, u32[]{:S(2)}) copy-start(bf16[256,512]{1,0:T(8,128)(2,1)} %o_ref.1) | copy-start | bytes 786436
  5.4 0.9 %copy-start.4 = (bf16[256,256]{1,0:T(8,128)(2,1)S(1)}, bf16[256,256]{1,0:T(8,128)(2,1)}, u32[]{:S(2)}) copy-start(bf16[256,256]{1,0:T(8,128)(2,1)} %q_ref.1) | copy-start | bytes 393220
  6.3 0.9 %copy-start.5 = (bf16[256,256]{1,0:T(8,128)(2,1)S(1)}, bf16[256,256]{1,0:T(8,128)(2,1)}, u32[]{:S(2)}) copy-start(bf16[256,256]{1,0:T(8,128)(2,1)} %k_ref.1) | copy-start | bytes 393220

commit v3 on v2

v3 whole, which is shorter than its diff:
```python
import functools

import jax
import jax.numpy as jnp
from jax import lax
from jax.experimental import pallas as pl
from jax.experimental.pallas import tpu as pltpu
from jax.sharding import PartitionSpec as P

DK = 128
DV = 256
BLOCK = 32
F32 = jnp.float32
BF16 = jnp.bfloat16
MESH = pl.DeviceIdType.MESH


def nn(left, right):
    return lax.dot_general(left, right, (((1,), (0,)), ((), ())), preferred_element_type=F32)


def nt(left, right):
    return lax.dot_general(left, right, (((1,), (1,)), ((), ())), preferred_element_type=F32)


def tn(left, right):
    return lax.dot_general(left, right, (((0,), (0,)), ((), ())), preferred_element_type=F32)


def pieces(value, count):
    parts = []
    for _ in range(count):
        part = value.astype(BF16)
        parts.append(part)
        value = value - part.astype(F32)
    return parts


def ring_place(z, x, nz, nx):
    r = nz - 1 - z
    across = jnp.where(r % 2 == 0, x - 1, nx - 1 - x)
    return jnp.where(x == 0, z, nz + r * (nx - 1) + across)


def ring_member(p, nz, nx):
    u = jnp.maximum(p - nz, 0)
    r = u // (nx - 1)
    w = u % (nx - 1)
    x = jnp.where(r % 2 == 0, 1 + w, nx - 1 - w)
    return jnp.where(p < nz, p * nx, (nz - 1 - r) * nx + x)


def kernel(
    n, nx, ntp,
    x_hbm, q_hbm, k_hbm, w_hbm, g_hbm, o_hbm,
    dq_ref, dk_ref, dg_ref, dw_ref, rn_ref,
    x_ref, q_ref, k_ref, w_ref, g_ref, o_ref, in_sem,
    c_buf, span_buf, v_buf, qg_buf, kt_buf, ks_buf, y_buf, kp_buf, vp_buf, st_buf, xt_buf, vg_buf,
    a_out, a_in, z_out, z_in, z_acc, c_out, c_in, h_out, h_in, b_out, b_in, fr_buf,
    first, part, ring, norm_out, norm_in,
    a_send, a_recv, z_send, z_recv, c_send, c_recv, h_send, h_recv, b_send, b_recv, r_send, r_recv, n_send, n_recv,
):
    nz = n // nx
    me = lax.axis_index("sp")
    mine = lax.axis_index("tp")
    z, x = me // nx, me % nx
    tokens, heads = q_ref.shape[0], q_ref.shape[1] // DK
    blocks = tokens // BLOCK
    dvx = DV // nx
    scale = DK ** (-0.5)
    loads = [
        pltpu.make_async_copy(source, target, in_sem.at[i])
        for i, (source, target) in enumerate(
            [(g_hbm, g_ref), (q_hbm, q_ref), (o_hbm, o_ref), (k_hbm, k_ref), (x_hbm, x_ref), (w_hbm, w_ref)]
        )
    ]
    for load in loads:
        load.start()
    barrier = pltpu.get_barrier_semaphore()
    for off in range(1, nx):
        pl.semaphore_signal(
            barrier, inc=1, device_id={"sp": z * nx + (x + off) % nx}, device_id_type=MESH)
    for off in range(1, nz):
        pl.semaphore_signal(
            barrier, inc=1, device_id={"sp": (z + off) % nz * nx + x}, device_id_type=MESH)
    for off in range(1, ntp):
        pl.semaphore_signal(barrier, inc=1, device_id={"tp": (mine + off) % ntp}, device_id_type=MESH)

    row = lax.broadcasted_iota(jnp.int32, (tokens, tokens), 0)
    col = lax.broadcasted_iota(jnp.int32, (tokens, tokens), 1)
    below = col <= row
    inside = below & (col // BLOCK == row // BLOCK)
    tri = jnp.where(below, 1.0, 0.0).astype(BF16)
    tri_in = jnp.where(inside, 1.0, 0.0).astype(BF16)
    upper = jnp.where(col >= row, 1.0, 0.0).astype(BF16)
    last_in = jnp.where(col // BLOCK == row // BLOCK, 1.0, 0.0).astype(BF16)

    def hd(h):
        return slice(h * DK, (h + 1) * DK)

    def hv(h):
        return slice(h * DV, (h + 1) * DV)

    loads[0].wait()
    g_parts = pieces(g_ref[...], 3)
    span_buf[...] = sum(nn(tri, part_) for part_ in g_parts)
    c_buf[...] = sum(nn(tri_in, part_) for part_ in g_parts)
    total = span_buf[tokens - 1 : tokens, :]
    decay = jnp.exp(total)

    def scatter_copy(d, m, h):
        return pltpu.make_async_remote_copy(
            src_ref=a_out.at[d, m, h], dst_ref=a_in.at[d, x, h],
            send_sem=a_send.at[d, m, h], recv_sem=a_recv.at[d, x, h],
            device_id={"sp": z * nx + m}, device_id_type=MESH)

    def scatter_wait(d, h):
        for m in range(nx):
            @pl.when(m != x)
            def _():
                pltpu.make_async_remote_copy(
                    src_ref=a_out.at[d, m, h], dst_ref=a_in.at[d, m, h],
                    send_sem=a_send.at[d, m, h], recv_sem=a_recv.at[d, m, h],
                    device_id={"sp": z * nx + m}, device_id_type=MESH).wait_recv()

    def give(d, h, totals):
        for m in range(nx):
            a_out[d, m, h, :dvx, :] = totals[m * dvx : (m + 1) * dvx]
            a_out[d, m, h, dvx:, :] = jnp.broadcast_to(decay[:, hd(h)], (8, DK))
        for m in range(nx):
            @pl.when(m != x)
            def _():
                scatter_copy(d, m, h).start()

            @pl.when(m == x)
            def _():
                a_in[d, m, h] = a_out[d, m, h]

    loads[1].wait()
    q_all = q_ref[...].astype(F32) * scale
    q_span = (q_all * jnp.exp(span_buf[...])).astype(BF16)
    loads[2].wait()
    for h in range(heads):
        adjoint = tn(o_ref[:, hv(h)], q_span[:, hd(h)])
        if h == 0:
            pl.semaphore_wait(barrier, nx - 1 + nz - 1 + ntp - 1)
        give(1, h, adjoint)

    for load in loads[3:]:
        load.wait()
    k_all = k_ref[...].astype(F32)
    k_far = jnp.exp(total - span_buf[...])
    k_span = (k_all * k_far).astype(BF16)
    for h in range(heads):
        v_buf[:, hv(h)] = nn(x_ref[...], w_ref[:, hv(h)]).astype(BF16)
        give(0, h, tn(v_buf[:, hv(h)], k_span[:, hd(h)]))

    def order(d):
        return range(nx) if d == 0 else range(nx - 1, -1, -1)

    def plane_copy(dz):
        return pltpu.make_async_remote_copy(
            src_ref=z_out, dst_ref=z_in.at[z],
            send_sem=z_send.at[dz], recv_sem=z_recv.at[z],
            device_id={"sp": (z + dz) * nx + x}, device_id_type=MESH)

    def composite(d, h, rows_):
        acc, dec = None, None
        for m in order(d):
            local, rate = a_in[d, m, h, rows_, :], a_in[d, m, h, dvx : dvx + 1, :]
            acc = local if acc is None else local + rate * acc
            dec = rate if dec is None else rate * dec
        return acc, dec

    for h in range(heads):
        scatter_wait(1, h)

    def forward_start():
        for h in range(heads):
            scatter_wait(0, h)
            acc, dec = composite(0, h, slice(0, dvx))
            z_out[h, :dvx, :] = acc
            z_out[h, dvx:, :] = jnp.broadcast_to(dec, (8, DK))
        for dz in range(1, nz):
            @pl.when(z + dz < nz)
            def _():
                plane_copy(dz).start()

    @pl.when(z < nz - 1)
    def _():
        forward_start()

    half_v = dvx // 2

    def chain_copy(c):
        return pltpu.make_async_remote_copy(
            src_ref=h_out.at[c], dst_ref=h_in.at[c],
            send_sem=h_send.at[c], recv_sem=h_recv.at[c],
            device_id={"sp": (z - 1) * nx + x}, device_id_type=MESH)

    def piece_copy(m, c):
        return pltpu.make_async_remote_copy(
            src_ref=b_out.at[m, c], dst_ref=b_in.at[x, c],
            send_sem=b_send.at[m, c], recv_sem=b_recv.at[x, c],
            device_id={"sp": z * nx + m}, device_id_type=MESH)

    for c in range(2 * heads):
        h, rows_ = c // 2, slice(c % 2 * half_v, (c % 2 + 1) * half_v)
        acc, dec = composite(1, h, rows_)

        @pl.when(z == nz - 1)
        def _():
            h_in[c] = jnp.zeros((half_v, DK), F32)

        @pl.when(z < nz - 1)
        def _():
            chain_copy(c).wait_recv()

        enter = h_in[c]

        @pl.when(z > 0)
        def _():
            h_out[c] = acc + dec * enter
            chain_copy(c).start()

        for m in order(1):
            b_out[m, c] = enter
            enter = a_in[1, m, h, rows_, :] + a_in[1, m, h, dvx : dvx + 1, :] * enter
        for m in range(nx):
            @pl.when(m != x)
            def _():
                piece_copy(m, c).start()

            @pl.when(m == x)
            def _():
                b_in[m, c] = b_out[m, c]

    @pl.when(z == nz - 1)
    def _():
        for h in range(heads):
            scatter_wait(0, h)

    cum = c_buf[...]
    block_end = sum(nn(last_in, part_) for part_ in g_parts)
    k_tail = jnp.exp(block_end - cum)
    grow = jnp.exp(cum)
    qg_buf[...] = (q_all * grow).astype(BF16)
    ks_buf[...] = (k_all * jnp.exp(-cum)).astype(BF16)
    kt_buf[...] = (k_all * k_tail).astype(BF16)
    st_buf[...] = jnp.zeros_like(st_buf)

    def adjoint_step(step, carry):
        rows = pl.ds(pl.multiple_of((blocks - 1 - step) * BLOCK, BLOCK), BLOCK)
        for h in range(heads):
            keep = jnp.exp(c_buf[rows, hd(h)][BLOCK - 1 :])
            adjoint = st_buf[1, h]
            narrow = adjoint.astype(BF16)
            kp_buf[rows, hd(h)] = nn(v_buf[rows, hv(h)], narrow)
            vp_buf[rows, hv(h)] = nt(kt_buf[rows, hd(h)], narrow)
            st_buf[1, h] = keep * adjoint + tn(o_ref[rows, hv(h)], qg_buf[rows, hd(h)])
        return carry

    def state_step(step, carry):
        rows = pl.ds(pl.multiple_of(step * BLOCK, BLOCK), BLOCK)
        for h in range(heads):
            keep = jnp.exp(c_buf[rows, hd(h)][BLOCK - 1 :])
            state = st_buf[0, h]
            y_buf[rows, hd(h)] = nn(o_ref[rows, hv(h)], state.astype(BF16))
            st_buf[0, h] = keep * state + tn(v_buf[rows, hv(h)], kt_buf[rows, hd(h)])
        return carry

    lax.fori_loop(0, blocks, adjoint_step, 0)

    for h in range(heads):
        dots = jnp.where(inside, nt(qg_buf[:, hd(h)], ks_buf[:, hd(h)]), 0.0).astype(BF16)
        vp_buf[:, hv(h)] += tn(dots, o_ref[:, hv(h)])

    depth = x_ref.shape[1]
    for at in range(0, depth, 256):
        xt_buf[at : at + 256, :] = x_ref[:, at : at + 256].T

    def member_copy(m):
        return pltpu.make_async_remote_copy(
            src_ref=c_out.at[m], dst_ref=c_in.at[x],
            send_sem=c_send.at[m], recv_sem=c_recv.at[x],
            device_id={"sp": z * nx + m}, device_id_type=MESH)

    def forward_spread():
        z_acc[...] = jnp.zeros_like(z_acc)
        for zp in range(nz):
            @pl.when(zp < z)
            def _():
                pltpu.make_async_remote_copy(
                    src_ref=z_out, dst_ref=z_in.at[zp],
                    send_sem=z_send.at[0], recv_sem=z_recv.at[zp],
                    device_id={"sp": zp * nx + x}, device_id_type=MESH).wait_recv()
                for h in range(heads):
                    z_acc[h] = z_in[zp, h, :dvx, :] + z_in[zp, h, dvx : dvx + 1, :] * z_acc[h]
        for h in range(heads):
            acc = z_acc[h]
            for m in order(0):
                c_out[m, h] = acc
                acc = a_in[0, m, h, :dvx, :] + a_in[0, m, h, dvx : dvx + 1, :] * acc
        for m in range(nx):
            @pl.when(m != x)
            def _():
                member_copy(m).start()

            @pl.when(m == x)
            def _():
                c_in[m] = c_out[m]

    for h in range(heads):
        for m in range(nx):
            for c in (2 * h, 2 * h + 1):
                @pl.when(m != x)
                def _():
                    pltpu.make_async_remote_copy(
                        src_ref=b_out.at[m, c], dst_ref=b_in.at[m, c],
                        send_sem=b_send.at[m, c], recv_sem=b_recv.at[m, c],
                        device_id={"sp": z * nx + m}, device_id_type=MESH).wait_recv()
                at = m * dvx + c % 2 * half_v
                fr_buf[h, at : at + half_v, :] = b_in[m, c]
        narrow = fr_buf[h].astype(BF16)
        vg_buf[:, hv(h)] = (vp_buf[:, hv(h)] + nt(k_span[:, hd(h)], narrow)).astype(BF16)

    own = dw_ref.shape[0]
    half_r, half_c = own // 2, dw_ref.shape[1] // 2
    p = ring_place(z, x, nz, nx)
    ahead = ring_member((p + 1) % n, nz, nx)
    behind = ring_member((p + n - 1) % n, nz, nx)

    def share(d, u, owner):
        rows_ = pl.ds(pl.multiple_of(owner * own + u * half_r, half_r), half_r)
        return nn(xt_buf[rows_, :], vg_buf[:, d * half_c : (d + 1) * half_c])

    def ring_copy(step, d, u, src):
        return pltpu.make_async_remote_copy(
            src_ref=src, dst_ref=ring.at[step, d, u],
            send_sem=r_send.at[step, d, u], recv_sem=r_recv.at[step, d, u],
            device_id={"sp": ahead if d == 0 else behind}, device_id_type=MESH)

    def owner_at(step, d):
        return ring_member((p + n - step - 1) % n if d == 0 else (p + step + 1) % n, nz, nx)

    for u in range(2):
        for d in range(2):
            first[d, u] = share(d, u, owner_at(0, d))
            ring_copy(0, d, u, first.at[d, u]).start()

    lax.fori_loop(0, blocks, state_step, 0)
    for h in range(heads):
        dots = jnp.where(inside, nt(o_ref[:, hv(h)], v_buf[:, hv(h)]), 0.0).astype(BF16)
        y_buf[:, hd(h)] += nn(dots, ks_buf[:, hd(h)])
        k_grad = (
            k_tail[:, hd(h)] * kp_buf[:, hd(h)]
            + jnp.exp(-cum[:, hd(h)]) * tn(dots, qg_buf[:, hd(h)])
            + k_far[:, hd(h)] * nn(v_buf[:, hv(h)], fr_buf[h].astype(BF16))
        )
        kp_buf[:, hd(h)] = k_grad
        dk_ref[:, hd(h)] = k_grad.astype(BF16)
    forward_spread()

    def query_side():
        for m in range(nx):
            @pl.when(m != x)
            def _():
                pltpu.make_async_remote_copy(
                    src_ref=c_out.at[m], dst_ref=c_in.at[m],
                    send_sem=c_send.at[m], recv_sem=c_recv.at[m],
                    device_id={"sp": z * nx + m}, device_id_type=MESH).wait_recv()
        for h in range(heads):
            state_in = jnp.concatenate([c_in[m, h] for m in range(nx)], axis=0)
            q_side = q_ref[:, hd(h)].astype(F32) * scale
            k_side = k_ref[:, hd(h)].astype(F32)
            q_grad = jnp.exp(c_buf[:, hd(h)]) * y_buf[:, hd(h)] + jnp.exp(span_buf[:, hd(h)]) * nn(
                o_ref[:, hv(h)], state_in.astype(BF16)
            )
            dq_ref[:, hd(h)] = (q_grad * scale).astype(BF16)
            terms = q_side * q_grad - k_side * kp_buf[:, hd(h)]
            far = jnp.exp(span_buf[tokens - 1 : tokens, hd(h)])
            span_end = st_buf[0, h] + far * state_in
            carry = jnp.sum(fr_buf[h] * span_end, axis=0, keepdims=True)
            dg_ref[:, hd(h)] = sum(nn(upper, part_) for part_ in pieces(terms, 3)) + carry

    def ring_step(step, carry):
        for d in range(2):
            for u in range(2):
                part[d, u] = share(d, u, owner_at(step, d))
        for u in range(2):
            for d in range(2):
                ring_copy(step - 1, d, u, first.at[d, u]).wait_recv()
                ring[step - 1, d, u] += part[d, u]
                ring_copy(step, d, u, ring.at[step - 1, d, u]).start()

        @pl.when(step == 2)
        def _():
            query_side()

        return carry

    lax.fori_loop(1, n - 1, ring_step, 0)

    for d in range(2):
        for u in range(2):
            part[d, u] = share(d, u, me)
    for u in range(2):
        squares = 0.0
        for d in range(2):
            ring_copy(n - 2, d, u, first.at[d, u]).wait_recv()
            done = ring[n - 2, d, u] + part[d, u]
            dw_ref[u * half_r : (u + 1) * half_r, d * half_c : (d + 1) * half_c] = done
            for at in range(0, half_c, 128):
                squares = squares + done[:, at : at + 128] * done[:, at : at + 128]
        norm_out[u] = jnp.broadcast_to(jnp.sum(squares.T, axis=0, keepdims=True), (8, half_r))

    def norm_copy(off):
        return pltpu.make_async_remote_copy(
            src_ref=norm_out, dst_ref=norm_in.at[off],
            send_sem=n_send.at[off], recv_sem=n_recv.at[off],
            device_id={"tp": (mine + off) % ntp}, device_id_type=MESH)

    for off in range(1, ntp):
        norm_copy(off).start()

    for m in range(nx):
        @pl.when(m != x)
        def _():
            for h in range(heads):
                for d in range(2):
                    scatter_copy(d, m, h).wait_send()
            for c in range(2 * heads):
                piece_copy(m, c).wait_send()
            member_copy(m).wait_send()
    for dz in range(1, nz):
        @pl.when(z + dz < nz)
        def _():
            plane_copy(dz).wait_send()

    @pl.when(z > 0)
    def _():
        for c in range(2 * heads):
            chain_copy(c).wait_send()

    def sent(step, carry):
        for u in range(2):
            for d in range(2):
                ring_copy(step, d, u, first.at[d, u]).wait_send()
        return carry

    lax.fori_loop(0, n - 1, sent, 0)
    norms = norm_out[...]
    for off in range(1, ntp):
        norm_copy(off).wait()
        norms = norms + norm_in[off]
    rn_ref[...] = norms


def finish(*refs):
    for source, target in zip(refs[:4], refs[5:9]):
        target[...] = source[...]
    refs[9][...] = refs[4][:, :1]


def on_device(n, nx, ntp, block_input, queries, keys, w_value, log_decay, d_out):
    tokens, wide = queries.shape
    heads = wide // DK
    cols = w_value.shape[1]
    depth = block_input.shape[1]
    own = depth // n
    nz = n // nx
    dvx = DV // nx
    vm = pltpu.VMEM
    dma = pltpu.SemaphoreType.DMA
    out = pl.pallas_call(
        functools.partial(kernel, n, nx, ntp),
        out_shape=(
            jax.ShapeDtypeStruct((tokens, wide), BF16),
            jax.ShapeDtypeStruct((tokens, wide), BF16),
            jax.ShapeDtypeStruct((tokens, wide), F32),
            jax.ShapeDtypeStruct((own, cols), F32),
            jax.ShapeDtypeStruct((2, 8, own // 2), F32),
        ),
        in_specs=[pl.BlockSpec(memory_space=pltpu.HBM)] * 6,
        out_specs=(pl.BlockSpec(memory_space=vm),) * 5,
        scratch_shapes=[
            vm(block_input.shape, BF16),
            vm(queries.shape, BF16),
            vm(keys.shape, BF16),
            vm(w_value.shape, BF16),
            vm(log_decay.shape, F32),
            vm(d_out.shape, BF16),
            dma((6,)),
            vm((tokens, wide), F32),
            vm((tokens, wide), F32),
            vm((tokens, cols), BF16),
            vm((tokens, wide), BF16),
            vm((tokens, wide), BF16),
            vm((tokens, wide), BF16),
            vm((tokens, wide), F32),
            vm((tokens, wide), F32),
            vm((tokens, cols), F32),
            vm((2, heads, DV, DK), F32),
            vm((depth, tokens), BF16),
            vm((tokens, cols), BF16),
            vm((2, nx, heads, dvx + 8, DK), F32),
            vm((2, nx, heads, dvx + 8, DK), F32),
            vm((heads, dvx + 8, DK), F32),
            vm((nz, heads, dvx + 8, DK), F32),
            vm((heads, dvx, DK), F32),
            vm((nx, heads, dvx, DK), F32),
            vm((nx, heads, dvx, DK), F32),
            vm((2 * heads, dvx // 2, DK), F32),
            vm((2 * heads, dvx // 2, DK), F32),
            vm((nx, 2 * heads, dvx // 2, DK), F32),
            vm((nx, 2 * heads, dvx // 2, DK), F32),
            vm((heads, DV, DK), F32),
            vm((2, 2, own // 2, cols // 2), F32),
            vm((2, 2, own // 2, cols // 2), F32),
            vm((n - 1, 2, 2, own // 2, cols // 2), F32),
            vm((2, 8, own // 2), F32),
            vm((ntp, 2, 8, own // 2), F32),
            dma((2, nx, heads)),
            dma((2, nx, heads)),
            dma((nz,)),
            dma((nz,)),
            dma((nx,)),
            dma((nx,)),
            dma((2 * heads,)),
            dma((2 * heads,)),
            dma((nx, 2 * heads)),
            dma((nx, 2 * heads)),
            dma((n - 1, 2, 2)),
            dma((n - 1, 2, 2)),
            dma((ntp,)),
            dma((ntp,)),
        ],
        compiler_params=pltpu.CompilerParams(
            collective_id=0, has_side_effects=True, vmem_limit_bytes=60 * 1024 * 1024
        ),
    )(block_input, queries, keys, w_value, log_decay, d_out)
    final = pl.pallas_call(
        finish,
        out_shape=tuple(jax.ShapeDtypeStruct(a.shape, a.dtype) for a in out[:4])
        + (jax.ShapeDtypeStruct((2, 1, own // 2), F32),),
        in_specs=[pl.BlockSpec(memory_space=vm)] * 5,
        out_specs=(pl.BlockSpec(memory_space=vm),) * 5,
        compiler_params=pltpu.CompilerParams(vmem_limit_bytes=60 * 1024 * 1024),
    )(*out)
    return (*final[:4], final[4].reshape(-1))


def solution(mesh):
    n, ntp = mesh.shape["sp"], mesh.shape["tp"]
    nx = 1 << ((n.bit_length() - 1) // 2)
    placed = (
        P("sp", None),
        P("sp", "tp"),
        P("sp", "tp"),
        P(None, "tp"),
        P("sp", "tp"),
        P("sp", "tp"),
    )
    return jax.shard_map(
        functools.partial(on_device, n, nx, ntp),
        mesh=mesh,
        in_specs=placed,
        out_specs=(P("sp", "tp"), P("sp", "tp"), P("sp", "tp"), P("sp", "tp"), P("sp")),
        check_vma=False,
    )
```

time: 81.4 us -> 75 us (0.921)
  local copies, waits for them, and re-layouts: 6.51 us -> 0 us
    unnamed x12 -> x0, local copies, waits for them, and re-layouts: 6.51 us -> none
    pallas_call x1, Pallas kernels: 1.03 us -> 2.2 us  [on_device(): pl.pallas_call(finish, out_shape=tuple((jax.ShapeDtypeStruct(a.shape, a.d...]
    pallas_call x1, Pallas kernels: 72.9 us -> 72 us  [on_device(): pl.pallas_call(functools.partial(kernel, n, nx, ntp), out_shape=(jax.Shap...]
where the time goes in v3:
time: 75 us; the launch traced here: 74.9 us
  Pallas kernels  74.2 us (99%)
    pallas_call x1, Pallas kernels, on_device(): pl.pallas_call(functools.partial(kernel, n, nx, ntp), out_shape=(jax.Shap...  72 us
    pallas_call x1, Pallas kernels, on_device(): pl.pallas_call(finish, out_shape=tuple((jax.ShapeDtypeStruct(a.shape, a.d...  2.2 us

profile of v3, /device:TPU:0, one launch (start us, length us, event | category | flops | bytes accessed | tf_op | source)
XLA Modules:
  0.0 74.9 jit_solution(5813061974935421348)
XLA Ops:
  0.6 72.0 %shard_map.101 = (bf16[256,256]{1,0:T(8,128)(2,1)}, bf16[256,256]{1,0:T(8,128)(2,1)}, f32[256,256]{1,0:T(8,128)}, f32[256,512]{1,0:T(8,128)}, f32[2,8,128]{2,1,0:T(8,128)}) custom-call(bf16[256,2048]{1,0:T(8,128)(2,1)} %x_hbm.1, bf16[256,256]{1,0:T(8,128)(2,1)} %q_hbm.1, bf16[256,256]{1,0:T(8,128)(2,1)} %k_hbm.1, bf16[2048,512]{1,0:T(8,128)(2,1)} %w_hbm.1, ...), custom_call_target="tpu_custom_call" | custom-call | tf_op jit(solution)/shard_map/pallas_call | solution.py:475
  72.7 2.2 %shard_map.102 = (bf16[256,256]{1,0:T(8,128)(2,1)}, bf16[256,256]{1,0:T(8,128)(2,1)}, f32[256,256]{1,0:T(8,128)}, f32[256,512]{1,0:T(8,128)}, f32[2,1,128]{2,1,0:T(1,128)}) custom-call(bf16[256,256]{1,0:T(8,128)(2,1)} %get-tuple-element.15.refs_0_, bf16[256,256]{1,0:T(8,128)(2,1)} %get-tuple-element.16.refs_1_, f32[256,256]{1,0:T(8,128)} %get-tuple-element.17.refs_2_, ...), custom_call_target="tpu_custom_call" | custom-call | tf_op jit(solution)/shard_map/pallas_call | solution.py:542

commit v4 on v3

--- a/solution.py
+++ b/solution.py
@@ -172,9 +172,6 @@
             dec = rate if dec is None else rate * dec
         return acc, dec
 
-    for h in range(heads):
-        scatter_wait(1, h)
-
     def forward_start():
         for h in range(heads):
             scatter_wait(0, h)
@@ -190,7 +187,7 @@
     def _():
         forward_start()
 
-    half_v = dvx // 2
+    half_v = dvx // 4
 
     def chain_copy(c):
         return pltpu.make_async_remote_copy(
@@ -204,8 +201,10 @@
             send_sem=b_send.at[m, c], recv_sem=b_recv.at[x, c],
             device_id={"sp": z * nx + m}, device_id_type=MESH)
 
-    for c in range(2 * heads):
-        h, rows_ = c // 2, slice(c % 2 * half_v, (c % 2 + 1) * half_v)
+    for c in range(4 * heads):
+        h, rows_ = c // 4, slice(c % 4 * half_v, (c % 4 + 1) * half_v)
+        if c % 4 == 0:
+            scatter_wait(1, h)
         acc, dec = composite(1, h, rows_)
 
         @pl.when(z == nz - 1)
@@ -312,14 +311,14 @@
 
     for h in range(heads):
         for m in range(nx):
-            for c in (2 * h, 2 * h + 1):
+            for c in range(4 * h, 4 * (h + 1)):
                 @pl.when(m != x)
                 def _():
                     pltpu.make_async_remote_copy(
                         src_ref=b_out.at[m, c], dst_ref=b_in.at[m, c],
                         send_sem=b_send.at[m, c], recv_sem=b_recv.at[m, c],
                         device_id={"sp": z * nx + m}, device_id_type=MESH).wait_recv()
-                at = m * dvx + c % 2 * half_v
+                at = m * dvx + c % 4 * half_v
                 fr_buf[h, at : at + half_v, :] = b_in[m, c]
         narrow = fr_buf[h].astype(BF16)
         vg_buf[:, hv(h)] = (vp_buf[:, hv(h)] + nt(k_span[:, hd(h)], narrow)).astype(BF16)
@@ -429,7 +428,7 @@
             for h in range(heads):
                 for d in range(2):
                     scatter_copy(d, m, h).wait_send()
-            for c in range(2 * heads):
+            for c in range(4 * heads):
                 piece_copy(m, c).wait_send()
             member_copy(m).wait_send()
     for dz in range(1, nz):
@@ -439,7 +438,7 @@
 
     @pl.when(z > 0)
     def _():
-        for c in range(2 * heads):
+        for c in range(4 * heads):
             chain_copy(c).wait_send()
 
     def sent(step, carry):
@@ -510,10 +509,10 @@
             vm((heads, dvx, DK), F32),
             vm((nx, heads, dvx, DK), F32),
             vm((nx, heads, dvx, DK), F32),
-            vm((2 * heads, dvx // 2, DK), F32),
-            vm((2 * heads, dvx // 2, DK), F32),
-            vm((nx, 2 * heads, dvx // 2, DK), F32),
-            vm((nx, 2 * heads, dvx // 2, DK), F32),
+            vm((4 * heads, dvx // 4, DK), F32),
+            vm((4 * heads, dvx // 4, DK), F32),
+            vm((nx, 4 * heads, dvx // 4, DK), F32),
+            vm((nx, 4 * heads, dvx // 4, DK), F32),
             vm((heads, DV, DK), F32),
             vm((2, 2, own // 2, cols // 2), F32),
             vm((2, 2, own // 2, cols // 2), F32),
@@ -526,10 +525,10 @@
             dma((nz,)),
             dma((nx,)),
             dma((nx,)),
-            dma((2 * heads,)),
-            dma((2 * heads,)),
-            dma((nx, 2 * heads)),
-            dma((nx, 2 * heads)),
+            dma((4 * heads,)),
+            dma((4 * heads,)),
+            dma((nx, 4 * heads)),
+            dma((nx, 4 * heads)),
             dma((n - 1, 2, 2)),
             dma((n - 1, 2, 2)),
             dma((ntp,)),

time: 75 us -> 73 us (0.973)
  Pallas kernels: 74.2 us -> 72.2 us
    pallas_call x1, Pallas kernels: 72 us -> 70 us  [on_device(): pl.pallas_call(functools.partial(kernel, n, nx, ntp), out_shape=(jax.Shap...]
where the time goes in v4:
time: 73 us; the launch traced here: 72.8 us
  Pallas kernels  72.2 us (99%)
    pallas_call x1, Pallas kernels, on_device(): pl.pallas_call(functools.partial(kernel, n, nx, ntp), out_shape=(jax.Shap...  70 us
    pallas_call x1, Pallas kernels, on_device(): pl.pallas_call(finish, out_shape=tuple((jax.ShapeDtypeStruct(a.shape, a.d...  2.2 us

profile of v4, /device:TPU:0, one launch (start us, length us, event | category | flops | bytes accessed | tf_op | source)
XLA Modules:
  0.0 72.8 jit_solution(13334137566370162254)
XLA Ops:
  0.6 70.0 %shard_map.101 = (bf16[256,256]{1,0:T(8,128)(2,1)}, bf16[256,256]{1,0:T(8,128)(2,1)}, f32[256,256]{1,0:T(8,128)}, f32[256,512]{1,0:T(8,128)}, f32[2,8,128]{2,1,0:T(8,128)}) custom-call(bf16[256,2048]{1,0:T(8,128)(2,1)} %x_hbm.1, bf16[256,256]{1,0:T(8,128)(2,1)} %q_hbm.1, bf16[256,256]{1,0:T(8,128)(2,1)} %k_hbm.1, bf16[2048,512]{1,0:T(8,128)(2,1)} %w_hbm.1, ...), custom_call_target="tpu_custom_call" | custom-call | tf_op jit(solution)/shard_map/pallas_call | solution.py:474
  70.6 2.2 %shard_map.102 = (bf16[256,256]{1,0:T(8,128)(2,1)}, bf16[256,256]{1,0:T(8,128)(2,1)}, f32[256,256]{1,0:T(8,128)}, f32[256,512]{1,0:T(8,128)}, f32[2,1,128]{2,1,0:T(1,128)}) custom-call(bf16[256,256]{1,0:T(8,128)(2,1)} %get-tuple-element.15.refs_0_, bf16[256,256]{1,0:T(8,128)(2,1)} %get-tuple-element.16.refs_1_, f32[256,256]{1,0:T(8,128)} %get-tuple-element.17.refs_2_, ...), custom_call_target="tpu_custom_call" | custom-call | tf_op jit(solution)/shard_map/pallas_call | solution.py:541
